TPU v7x, 32 devices: a whole 2x2x4 slice. The times are simulated.
32 devices in a mesh: ep: 32 (over z, y, x, core).
Axes of the slice: x: 2, y: 2, z: 4, core: 2. Of those that a mesh axis runs over, the one named last changes fastest.
Arguments:
- residual: bfloat16 [2048, 2048], P('ep'), may hold values from -6 to 6
- branch_in: bfloat16 [2048, 1024], P('ep'), may hold values from -6 to 6
- state_real: float32 [2048, 4096], P('ep'), may hold values from -4 to 4
- state_imag: float32 [2048, 4096], P('ep'), may hold values from -4 to 4
- decay_rate: float32 [64, 64], replicated, may hold values from 0.1 to 1
- frequency: float32 [64, 64], replicated, may hold values from 0 to 200
- log_step: float32 [64], replicated, may hold values from -4 to 0
- input_real: bfloat16 [64, 64, 16], replicated, may hold values from -1 to 1
- input_imag: bfloat16 [64, 64, 16], replicated, may hold values from -1 to 1
- output_matrix_real: bfloat16 [64, 16, 64], replicated, may hold values from -0.5 to 0.5
- output_matrix_imaginary: bfloat16 [64, 16, 64], replicated, may hold values from -0.5 to 0.5
- skip_gain: float32 [1024], replicated, may hold values from -4 to 4
- glu_value: bfloat16 [1024, 2048], replicated, may hold values from -0.1875 to 0.1875
- glu_gate: bfloat16 [1024, 2048], replicated, may hold values from -0.1875 to 0.1875
- mix_gain: float32 [2048], replicated, may hold values from 0.1 to 1.9
- moe_in_gain: float32 [2048], replicated, may hold values from 0.1 to 1.9
- moe_out_gain: float32 [2048], replicated, may hold values from 0.1 to 1.9
- routes: int32 [2048, 6], P('ep'), may hold values from 0 to 31, all different within a row; in each aligned block of 64 rows (0 to 63, 64 to 127, ...) at most 16 rows name the same one
- route_weights: float32 [2048, 6], P('ep'), may hold values from 0.05 to 0.6
- expert_gate: bfloat16 [32, 2048, 512], P('ep'), may hold values from -0.125 to 0.125
- expert_up: bfloat16 [32, 2048, 512], P('ep'), may hold values from -0.125 to 0.125
- expert_down: bfloat16 [32, 512, 2048], P('ep'), may hold values from -0.25 to 0.25
- shared_gate: bfloat16 [2048, 512], replicated, may hold values from -0.125 to 0.125
- shared_up: bfloat16 [2048, 512], replicated, may hold values from -0.125 to 0.125
- shared_down: bfloat16 [512, 2048], replicated, may hold values from -0.25 to 0.25
Outputs:
- layer_out: bfloat16 [2048, 2048], P('ep')
- next_real: float32 [2048, 4096], P('ep')
- next_imag: float32 [2048, 4096], P('ep')
Inputs may be any that keep to these rules, and one draw needn't show every extreme that they name: `routes`: among the rows of one device no expert is named more than 16 times, and in every draw some expert is named exactly 16 times by some device's rows; a token's experts are distinct.
All inputs are finite; a program needn't handle non-finite values.
Results may differ from a plain program's by a relative error of at most 0.0066.
Values may be sent and summed in bfloat16 or wider, within the bound.
A program may use at most 128 MiB of HBM per device.

v0:
```python
import jax
import jax.numpy as jnp
from jax import lax
from jax.sharding import PartitionSpec as P

norm_eps = 1e-06


def scaled_norm(row_block, norm_gain):
    return (
        row_block
        * lax.rsqrt(jnp.mean(row_block * row_block, axis=-1, keepdims=True) + norm_eps)
        * norm_gain
    )


def state_step(
    branch_in,
    state_real,
    state_imag,
    decay_rate,
    frequency,
    log_step,
    input_real,
    input_imag,
    output_matrix_real,
    output_matrix_imaginary,
    skip_gain,
):
    seq_count = branch_in.shape[0]
    group_count, state_count = decay_rate.shape
    chan_count = input_real.shape[2]
    step_size = jnp.exp(log_step)[:, None]
    magnitude = jnp.exp(-decay_rate * step_size)
    abar_re = magnitude * jnp.cos(frequency * step_size)
    abar_im = magnitude * jnp.sin(frequency * step_size)
    lam_re = -decay_rate
    denominator = lam_re * lam_re + frequency * frequency
    numer_re = abar_re - 1.0
    coef_re = (numer_re * lam_re + abar_im * frequency) / denominator
    coef_im = (abar_im * lam_re - numer_re * frequency) / denominator
    b_real = input_real.astype(jnp.float32)
    b_imag = input_imag.astype(jnp.float32)
    bbar_re = coef_re[..., None] * b_real - coef_im[..., None] * b_imag
    bbar_im = coef_re[..., None] * b_imag + coef_im[..., None] * b_real
    feed_rows = branch_in.astype(jnp.float32).reshape(seq_count, group_count, chan_count)
    forcing_real = jnp.einsum("tgc,gpc->tgp", feed_rows, bbar_re, precision=lax.Precision.HIGHEST)
    drive_im = jnp.einsum("tgc,gpc->tgp", feed_rows, bbar_im, precision=lax.Precision.HIGHEST)
    old_re = state_real.reshape(seq_count, group_count, state_count)
    old_im = state_imag.reshape(seq_count, group_count, state_count)
    fresh_real = abar_re * old_re - abar_im * old_im + forcing_real
    fresh_imaginary = abar_re * old_im + abar_im * old_re + drive_im
    state_readout = jnp.einsum(
        "ukb,krb->ukr",
        fresh_real,
        output_matrix_real.astype(jnp.float32),
        precision=lax.Precision.HIGHEST,
    ) - jnp.einsum(
        "ukb,krb->ukr",
        fresh_imaginary,
        output_matrix_imaginary.astype(jnp.float32),
        precision=lax.Precision.HIGHEST,
    )
    mixed_rows = state_readout.reshape(
        seq_count, group_count * chan_count
    ) + skip_gain * branch_in.astype(jnp.float32)
    activated = jax.nn.gelu(mixed_rows).astype(jnp.bfloat16)
    return (activated, fresh_real.reshape(seq_count, -1), fresh_imaginary.reshape(seq_count, -1))


def expert_rows(row_block, w_gate, w_up, w_down):
    gate_part = jnp.dot(row_block, w_gate, preferred_element_type=jnp.float32)
    up_part = jnp.dot(row_block, w_up, preferred_element_type=jnp.float32)
    hidden = (jax.nn.silu(gate_part) * up_part).astype(jnp.bfloat16)
    return jnp.dot(hidden, w_down, preferred_element_type=jnp.float32)


def mixer_residual(residual, activated, glu_value, glu_gate, mix_gain):
    value_part = jnp.dot(activated, glu_value, preferred_element_type=jnp.float32)
    gate_part = jnp.dot(activated, glu_gate, preferred_element_type=jnp.float32)
    branch = value_part * jax.nn.sigmoid(gate_part)
    return (residual.astype(jnp.float32) + scaled_norm(branch, mix_gain)).astype(jnp.bfloat16)


def serve_rows(
    residual, branch_in, state_real, state_imag, routes, route_weights, params, capacity
):
    (
        decay_rate,
        frequency,
        log_step,
        input_real,
        input_imag,
        output_matrix_real,
        output_matrix_imaginary,
        skip_gain,
        glu_value,
        glu_gate,
        mix_gain,
        moe_in_gain,
        moe_out_gain,
        expert_gate,
        expert_up,
        expert_down,
        shared_gate,
        shared_up,
        shared_down,
    ) = params
    activated, next_real, next_imag = state_step(
        branch_in,
        state_real,
        state_imag,
        decay_rate,
        frequency,
        log_step,
        input_real,
        input_imag,
        output_matrix_real,
        output_matrix_imaginary,
        skip_gain,
    )
    resid_mid = mixer_residual(residual, activated, glu_value, glu_gate, mix_gain)
    normed = scaled_norm(resid_mid.astype(jnp.float32), moe_in_gain).astype(jnp.bfloat16)
    seq_count, hidden_width = normed.shape
    top_count = routes.shape[1]
    expert_count = lax.axis_size("ep")
    flat_routes = routes.reshape(-1)
    assign_count = seq_count * top_count
    position = jnp.arange(assign_count, dtype=jnp.int32)
    earlier = (flat_routes[:, None] == flat_routes[None, :]) & (
        position[None, :] < position[:, None]
    )
    slot_rank = jnp.sum(earlier.astype(jnp.int32), axis=1)
    slot_index = flat_routes * capacity + slot_rank
    slot_source = (
        jnp.full((expert_count * capacity,), seq_count, jnp.int32)
        .at[slot_index]
        .set(position // top_count)
    )
    padded = jnp.concatenate([normed, jnp.zeros((1, hidden_width), jnp.bfloat16)], axis=0)
    outgoing = padded[slot_source].reshape(expert_count, capacity, hidden_width)
    received_rows = lax.all_to_all(outgoing, "ep", split_axis=0, concat_axis=0, tiled=True)
    source_count = received_rows.shape[0]
    item_count = received_rows.shape[1]
    produced = expert_rows(
        received_rows.reshape(-1, hidden_width), expert_gate[0], expert_up[0], expert_down[0]
    ).astype(jnp.bfloat16)
    returned = lax.all_to_all(
        produced.reshape(source_count, item_count, hidden_width),
        "ep",
        split_axis=0,
        concat_axis=0,
        tiled=True,
    )
    per_assign = (
        returned.reshape(-1, hidden_width)[slot_index]
        .reshape(seq_count, top_count, hidden_width)
        .astype(jnp.float32)
    )
    routed = jnp.sum(per_assign * route_weights[..., None], axis=1)
    shared = expert_rows(normed, shared_gate, shared_up, shared_down)
    combined = shared + routed
    layer_out = (resid_mid.astype(jnp.float32) + scaled_norm(combined, moe_out_gain)).astype(
        jnp.bfloat16
    )
    return (layer_out, next_real, next_imag)


def per_device(
    residual,
    branch_in,
    state_real,
    state_imag,
    decay_rate,
    frequency,
    log_step,
    input_real,
    input_imag,
    output_matrix_real,
    output_matrix_imaginary,
    skip_gain,
    glu_value,
    glu_gate,
    mix_gain,
    moe_in_gain,
    moe_out_gain,
    routes,
    route_weights,
    expert_gate,
    expert_up,
    expert_down,
    shared_gate,
    shared_up,
    shared_down,
):
    params = (
        decay_rate,
        frequency,
        log_step,
        input_real,
        input_imag,
        output_matrix_real,
        output_matrix_imaginary,
        skip_gain,
        glu_value,
        glu_gate,
        mix_gain,
        moe_in_gain,
        moe_out_gain,
        expert_gate,
        expert_up,
        expert_down,
        shared_gate,
        shared_up,
        shared_down,
    )
    seq_dev = residual.shape[0]
    capacity = max(2, 4 * seq_dev * routes.shape[1] // (3 * lax.axis_size("ep")))
    return serve_rows(
        residual, branch_in, state_real, state_imag, routes, route_weights, params, capacity
    )


def solution(mesh):
    return jax.shard_map(
        per_device,
        mesh=mesh,
        in_specs=(
            P("ep", None),
            P("ep", None),
            P("ep", None),
            P("ep", None),
            P(),
            P(),
            P(),
            P(),
            P(),
            P(),
            P(),
            P(),
            P(),
            P(),
            P(),
            P(),
            P(),
            P("ep", None),
            P("ep", None),
            P("ep", None, None),
            P("ep", None, None),
            P("ep", None, None),
            P(),
            P(),
            P(),
        ),
        out_specs=(P("ep", None), P("ep", None), P("ep", None)),
        check_vma=False,
    )
```

profile of v0, /device:TPU:17, one launch (start us, length us, event | category | flops | bytes accessed | tf_op | source)
XLA Modules:
  0.0 173.2 jit_solution(2688304391848498240)
XLA Ops:
  0.6 0.0 copy-start
  0.7 0.8 broadcast_multiply_fusion
  1.5 0.8 copy.56
  2.3 0.7 exp.17
  2.9 1.1 copy.51
  4.0 3.2 %copy.49 = f32[64,4096]{0,1:T(8,128)} copy(f32[64,4096]{1,0:T(8,128)} %param.27) | data formatting | bytes 2097152 | tf_op args[2]
  7.2 3.2 %copy.50 = f32[64,4096]{0,1:T(8,128)} copy(f32[64,4096]{1,0:T(8,128)} %param.28) | data formatting | bytes 2097152 | tf_op args[3]
  10.4 0.0 copy-done.13
  10.4 0.2 add_divide_fusion
  10.7 6.0 %bitcast_add_fusion = f32[64,64,64]{0,2,1:T(8,128)} fusion(f32[64,64,64]{0,2,1:T(8,128)} %bitcast.49, f32[64,64,64]{0,2,1:T(8,128)} %bitcast.51, bf16[64,64,16]{0,2,1:T(8,128)(2,1)S(1)} %bitcast.56, f32[64,64]{1,0:T(8,128)S(1)} %get-tuple-element.17, f32[64,64]{1,0:T(8,128)S(1)} %get-tuple-element.15, bf16[64,64,16]{1,2,0:T(8,128)(2,1)S(1)} %copy-done.6, ...), kind=kOutput, calls=%fused_computation.16 | convolution fusion | flops 51707904 | bytes 3604480 | tf_op jit(solution)/shard_map/tgc,gpc->tgp/dot_general | solution.py:48
  16.7 0.0 copy-done.2
  16.7 4.1 %bitcast_add_fusion.1 = f32[64,64,64]{0,2,1:T(8,128)} fusion(f32[64,64,64]{0,2,1:T(8,128)S(1)} %bitcast.52, f32[64,64,64]{0,2,1:T(8,128)S(1)} %bitcast.50, bf16[64,64,16]{0,2,1:T(8,128)(2,1)S(1)} %bitcast.57, f32[64,64]{1,0:T(8,128)S(1)} %get-tuple-element.17, f32[64,64]{1,0:T(8,128)S(1)} %get-tuple-element.15, bf16[64,64,16]{1,2,0:T(8,128)(2,1)S(1)} %copy-done.6, ...), kind=kOutput, calls=%fused_computation.17 | convolution fusion | flops 51707904 | bytes 3604480 | tf_op jit(solution)/shard_map/tgc,gpc->tgp/dot_general | solution.py:47
  20.8 0.1 copy.55
  20.8 0.1 mul.272
  21.0 0.1 eq.15
  21.1 0.2 convert_reduce_fusion
  21.4 2.9 %scatter_custom_fusion = s32[512]{0:T(512)S(1)} fusion(s32[384]{0:T(512)S(1)} %fusion.48, s32[384]{0:T(512)S(1)} %add_select_fusion, s32[]{:T(128)} %constant.14.clone.1), kind=kCustom, calls=%fused_computation.81 | custom fusion | bytes 2052 | tf_op jit(solution)/shard_map/scatter | solution.py:138
  24.4 2.8 %fusion.53 = f32[64,64,16]{1,2,0:T(8,128)S(1)} fusion(f32[64,64,64]{0,2,1:T(8,128)} %bitcast_add_fusion.1, bf16[64,16,64]{2,1,0:T(8,128)(2,1)S(1)} %copy-done.10), kind=kOutput, calls=%fused_computation.88 | convolution fusion | flops 50331648 | bytes 1441792 | tf_op jit(solution)/shard_map/ukb,krb->ukr/dot_general | solution.py:53
  27.2 0.0 copy-start.8
  27.2 0.0 copy-start.17
  27.2 1.1 convolution_subtract_fusion
  28.4 0.2 copy.54
  28.5 0.0 copy-done.8
  28.5 0.0 copy-done.17
  28.6 0.1 fusion.34
  28.7 0.0 copy-start.4
  28.7 3.2 %fusion.2 = f32[64,2048]{1,0:T(8,128)S(1)} fusion(bf16[64,1024]{1,0:T(8,128)(2,1)S(1)} %fusion.34, bf16[1024,2048]{1,0:T(8,128)(2,1)} %param.38), kind=kOutput, calls=%fused_computation.10 | convolution fusion | flops 268828672 | bytes 4849664 | tf_op jit(solution)/shard_map/dot_general | solution.py:80
  31.9 0.2 copy-done.4
  32.1 1.0 multiply_reduce_fusion.2
  33.1 0.3 fusion.22
  33.4 0.1 fusion.24
  33.6 3.3 %gather_fusion = bf16[512,2048]{1,0:T(8,128)(2,1)} fusion(bf16[65,2048]{1,0:T(8,128)(2,1)S(1)} %concatenate.3, s32[1024]{0:T(1024)S(1)} %pad_clamp_fusion.1), kind=kCustom, calls=%fused_computation | custom fusion | bytes 4196352 | tf_op jit(solution)/shard_map/gather | solution.py:141
  36.9 53.7 %all_to_all.10 = bf16[32,16,2048]{2,1,0:T(8,128)(2,1)S(1)} all-to-all(bf16[32,16,2048]{2,1,0:T(8,128)(2,1)} %bitcast.55), channel_id=1, replica_groups=mesh['ep'=32] {'ep'}, dimensions={0} | all-to-all | bytes 4194304 | tf_op jit(solution)/shard_map/all_to_all | solution.py:142
  90.6 1.3 copy-done.5
  91.9 2.2 %fusion.6 = f32[512,512]{1,0:T(8,128)} fusion(bf16[512,2048]{1,0:T(8,128)(2,1)S(1)} %bitcast.59, bf16[1,2048,512]{2,1,0:T(8,128)(2,1)S(1)} %copy-done.19), kind=kOutput, calls=%fused_computation.14 | convolution fusion | flops 1073741824 | bytes 5242880 | tf_op jit(solution)/shard_map/dot_general | solution.py:72
  94.1 6.3 %convolution_convert_fusion = bf16[512,2048]{1,0:T(8,128)(2,1)} fusion(bf16[1,512,2048]{2,1,0:T(8,128)(2,1)S(1)} %copy-done, bf16[512,2048]{1,0:T(8,128)(2,1)} %bitcast.60, bf16[1,2048,512]{2,1,0:T(8,128)(2,1)} %param.45, f32[512,512]{1,0:T(8,128)} %fusion.6), kind=kOutput, calls=%fused_computation.4 | convolution fusion | flops 2150105088 | bytes 9437184 | tf_op jit(solution)/shard_map/dot_general | solution.py:75
  100.4 4.9 %all-to-all-start.1 = ((bf16[32,16,2048]{2,1,0:T(8,128)(2,1)}), bf16[32,16,2048]{2,1,0:T(8,128)(2,1)}, u32[]{:S(2)}, u32[]{:S(2)}) async-start(bf16[32,16,2048]{2,1,0:T(8,128)(2,1)} %bitcast.58), calls=%async_computation.1 | async-start | bytes 4194304 | tf_op jit(solution)/shard_map/all_to_all | solution.py:148
  105.4 0.1 copy.57
  105.5 3.1 %copy.59 = f32[64,4096]{1,0:T(8,128)} copy(f32[64,4096]{0,1:T(8,128)} %bitcast.54) | data formatting | bytes 2097152
  108.6 3.1 %copy.58 = f32[64,4096]{1,0:T(8,128)} copy(f32[64,4096]{0,1:T(8,128)} %bitcast.53) | data formatting | bytes 2097152
  111.8 2.1 %fusion.54 = f32[64,512]{1,0:T(8,128)S(1)} fusion(bf16[64,2048]{1,0:T(8,128)(2,1)S(1)} %fusion.24, bf16[2048,512]{1,0:T(8,128)(2,1)} %param.47), kind=kOutput, calls=%fused_computation.89 | convolution fusion | flops 134217728 | bytes 2490368 | tf_op jit(solution)/shard_map/dot_general | solution.py:72
  113.8 38.8 %all-to-all-done.1 = bf16[32,16,2048]{2,1,0:T(8,128)(2,1)} async-done(((bf16[32,16,2048]{2,1,0:T(8,128)(2,1)}), bf16[32,16,2048]{2,1,0:T(8,128)(2,1)}, u32[]{:S(2)}, u32[]{:S(2)}) %all-to-all-start.1) | async-done | bytes 2097184 | tf_op jit(solution)/shard_map/all_to_all | solution.py:148
  152.6 6.9 %gather_fusion.1 = bf16[384,2048]{1,0:T(8,128)(2,1)} fusion(bf16[512,2048]{1,0:T(8,128)(2,1)} %bitcast.13, s32[1024]{0:T(1024)S(1)} %pad_clamp_fusion), kind=kCustom, calls=%fused_computation.1 | custom fusion | bytes 3147264 | tf_op jit(solution)/shard_map/gather | solution.py:156
  159.5 3.9 %reshape.114 = f32[64,6,2048]{2,1,0:T(8,128)} reshape(bf16[384,2048]{1,0:T(8,128)(2,1)} %gather_fusion.1) | data formatting | bytes 4718592 | tf_op jit(solution)/shard_map/convert_element_type | solution.py:158
  163.4 3.7 %multiply_reduce_fusion = f32[64,2048]{1,0:T(8,128)S(1)} fusion(f32[64,6,2048]{2,1,0:T(8,128)} %reshape.114, f32[64,6]{1,0:T(8,128)S(1)} %copy.57), kind=kLoop, calls=%fused_computation.3 | loop fusion | flops 1441792 | bytes 3671552 | tf_op jit(solution)/shard_map/reduce_sum | solution.py:160
  167.2 0.0 copy-start.16
  167.2 4.0 %multiply_reduce_fusion.1 = (f32[64]{0:T(128)S(1)}, f32[64,2048]{1,0:T(8,128)}) fusion(f32[64,2048]{1,0:T(8,128)S(1)} %multiply_reduce_fusion, bf16[512,2048]{1,0:T(8,128)(2,1)} %param.49, bf16[64,2048]{1,0:T(8,128)(2,1)S(1)} %fusion.24, bf16[2048,512]{1,0:T(8,128)(2,1)} %param.48, f32[64,512]{1,0:T(8,128)S(1)} %fusion.54), kind=kOutput, calls=%fused_computation.39 | convolution fusion | flops 269025216 | bytes 5636352 | tf_op jit(solution)/shard_map/dot_general | solution.py:75
  171.3 1.9 %fusion.25 = bf16[64,2048]{1,0:T(8,128)(2,1)} fusion(bf16[64,2048]{1,0:T(8,128)(2,1)S(1)} %get-tuple-element.13, f32[64,2048]{1,0:T(8,128)} %get-tuple-element.21, f32[2048]{0:T(1024)S(1)} %copy-done.16, f32[64]{0:T(128)S(1)} %add_rsqrt_fusion), kind=kLoop, calls=%fused_computation.38 | loop fusion | flops 655360 | bytes 1057024 | tf_op jit(solution)/shard_map/convert_element_type | solution.py:163
  (38 shorter events, 0.2 us)
Async XLA Ops:
  0.6 93.5 %copy-start = (bf16[1,512,2048]{2,1,0:T(8,128)(2,1)S(1)}, bf16[1,512,2048]{2,1,0:T(8,128)(2,1)}, u32[]{:S(2)}) copy-start(bf16[1,512,2048]{2,1,0:T(8,128)(2,1)} %param.46) | copy-start | bytes 6291460
  7.2 3.2 %copy-start.12 = (f32[64,64]{1,0:T(8,128)S(1)}, f32[64,64]{1,0:T(8,128)}, u32[]{:S(2)}) copy-start(f32[64,64]{1,0:T(8,128)} %param.30) | copy-start | bytes 49156
  7.2 3.2 %copy-start.13 = (f32[64,64]{1,0:T(8,128)S(1)}, f32[64,64]{1,0:T(8,128)}, u32[]{:S(2)}) copy-start(f32[64,64]{1,0:T(8,128)} %param.29) | copy-start | bytes 49156
  7.2 3.4 %copy-start.6 = (bf16[64,64,16]{1,2,0:T(8,128)(2,1)S(1)}, bf16[64,64,16]{1,2,0:T(8,128)(2,1)}, u32[]{:S(2)}) copy-start(bf16[64,64,16]{1,2,0:T(8,128)(2,1)} %param.32) | copy-start | bytes 393220
  7.2 3.5 %copy-start.7 = (bf16[64,64,16]{1,2,0:T(8,128)(2,1)S(1)}, bf16[64,64,16]{1,2,0:T(8,128)(2,1)}, u32[]{:S(2)}) copy-start(bf16[64,64,16]{1,2,0:T(8,128)(2,1)} %param.33) | copy-start | bytes 393220
  10.6 6.0 %copy-start.1 = (f32[64,4096]{0,1:T(8,128)S(1)}, f32[64,4096]{0,1:T(8,128)}, u32[]{:S(2)}) copy-start(f32[64,4096]{0,1:T(8,128)} %copy.49) | copy-start | bytes 3145732
  10.6 6.0 %copy-start.2 = (f32[64,4096]{0,1:T(8,128)S(1)}, f32[64,4096]{0,1:T(8,128)}, u32[]{:S(2)}) copy-start(f32[64,4096]{0,1:T(8,128)} %copy.50) | copy-start | bytes 3145732
  16.7 7.7 %copy-start.10 = (bf16[64,16,64]{2,1,0:T(8,128)(2,1)S(1)}, bf16[64,16,64]{2,1,0:T(8,128)(2,1)}, u32[]{:S(2)}) copy-start(bf16[64,16,64]{2,1,0:T(8,128)(2,1)} %param.34) | copy-start | bytes 393220
  20.8 6.5 %copy-start.11 = (bf16[64,16,64]{2,1,0:T(8,128)(2,1)S(1)}, bf16[64,16,64]{2,1,0:T(8,128)(2,1)}, u32[]{:S(2)}) copy-start(bf16[64,16,64]{2,1,0:T(8,128)(2,1)} %param.35) | copy-start | bytes 393220
  24.3 2.9 %copy-start.3 = (f32[64,64,64]{0,2,1:T(8,128)S(1)}, f32[64,64,64]{0,2,1:T(8,128)}, u32[]{:S(2)}) copy-start(f32[64,64,64]{0,2,1:T(8,128)} %bitcast_add_fusion) | copy-start | bytes 3145732
  27.2 1.3 copy-start.8
  27.2 1.3 copy-start.17
  28.7 3.5 %copy-start.4 = (bf16[1024,2048]{1,0:T(8,128)(2,1)S(1)}, bf16[1024,2048]{1,0:T(8,128)(2,1)}, u32[]{:S(2)}) copy-start(bf16[1024,2048]{1,0:T(8,128)(2,1)} %param.37) | copy-start | bytes 12582916
  32.1 1.0 copy-start.9
  32.1 1.0 copy-start.14
  32.1 1.3 copy-start.15
  36.9 55.0 %copy-start.19 = (bf16[1,2048,512]{2,1,0:T(8,128)(2,1)S(1)}, bf16[1,2048,512]{2,1,0:T(8,128)(2,1)}, u32[]{:S(2)}) copy-start(bf16[1,2048,512]{2,1,0:T(8,128)(2,1)} %param.44) | copy-start | bytes 6291460
  90.6 1.3 copy-start.5
  100.4 5.0 %copy-start.18 = (f32[64,6]{0,1:T(8,128)S(1)}, f32[64,6]{0,1:T(8,128)}, u32[]{:S(2)}) copy-start(f32[64,6]{0,1:T(8,128)} %param.43) | copy-start | bytes 4612
  100.4 52.2 %all-to-all-start.1 = ((bf16[32,16,2048]{2,1,0:T(8,128)(2,1)}), bf16[32,16,2048]{2,1,0:T(8,128)(2,1)}, u32[]{:S(2)}, u32[]{:S(2)}) async-start(bf16[32,16,2048]{2,1,0:T(8,128)(2,1)} %bitcast.58), calls=%async_computation.1 | async-start | bytes 4194304 | tf_op jit(solution)/shard_map/all_to_all | solution.py:148
  167.2 4.1 %copy-start.16 = (f32[2048]{0:T(1024)S(1)}, f32[2048]{0:T(1024)}, u32[]{:S(2)}) copy-start(f32[2048]{0:T(1024)} %param.41) | copy-start | bytes 24580
where the time goes:
time: 176 us; the launch traced here: 173 us
  blocking collectives  53.7 us (31%)
  waiting for transfers between devices  38.8 us (22%)
  local copies, waits for them, and re-layouts  34.5 us (20%)
  matrix products  32.8 us (19%)
  other arithmetic  7.54 us (4%)
  starting transfers between devices  4.95 us (3%)
    all_to_all x1, blocking collectives, serve_rows(): lax.all_to_all(outgoing, 'ep', split_axis=0, concat_axis=0, tiled=True)  53.7 us
    all_to_all x1, waiting for transfers between devices, serve_rows(): lax.all_to_all(produced.reshape(source_count, item_count, hidden_width),...  38.8 us
    unnamed x47, local copies, waits for them, and re-layouts  16.2 us
    dot_general x2, matrix products, expert_rows(): return jnp.dot(hidden, w_down, preferred_element_type=jnp.float32)  10.3 us
    gather x1, local copies, waits for them, and re-layouts, serve_rows(): returned.reshape(-1, hidden_width)[slot_index]  6.9 us
    dot_general x1, matrix products, state_step(): jnp.einsum('tgc,gpc->tgp', feed_rows, bbar_im, precision=lax.Precision.HI...  6.02 us
    all_to_all x1, starting transfers between devices, serve_rows(): lax.all_to_all(produced.reshape(source_count, item_count, hidden_width),...  4.95 us
    dot_general x2, matrix products, expert_rows(): gate_part = jnp.dot(row_block, w_gate, preferred_element_type=jnp.float32)  4.28 us
  transfers between devices with their start and end apart: 1, of which 1 were waited for; matrix products, arithmetic and copies ran while one was open for 5% of the time, Pallas kernels for 0%

commit v1 on v0

--- a/solution.py
+++ b/solution.py
@@ -1,9 +1,15 @@
+import functools
+
 import jax
 import jax.numpy as jnp
 from jax import lax
+from jax.experimental import pallas as pl
+from jax.experimental.pallas import tpu as pltpu
 from jax.sharding import PartitionSpec as P
 
 norm_eps = 1e-06
+ROW_TILE = 16
+MESH = pl.DeviceIdType.MESH
 
 
 def scaled_norm(row_block, norm_gain):
@@ -12,6 +18,268 @@
         * lax.rsqrt(jnp.mean(row_block * row_block, axis=-1, keepdims=True) + norm_eps)
         * norm_gain
     )
+
+
+def flipped(index, mask):
+    out, bit = 0, 1
+    while bit <= mask or bit == 1:
+        digit = (index // bit) % 2
+        out = out + bit * ((digit + 1) % 2 if mask & bit else digit)
+        bit *= 2
+    return out + (index // bit) * bit
+
+
+def moe_kernel(
+    planes,
+    width,
+    cap,
+    normed,
+    resid,
+    slot_weights,
+    out_gain,
+    eg_hbm,
+    eu_hbm,
+    ed_hbm,
+    sg_hbm,
+    su_hbm,
+    sd_hbm,
+    out,
+    eg,
+    eu,
+    ed,
+    sg,
+    su,
+    sd,
+    col_rows,
+    col_weights,
+    x_send,
+    x_recv,
+    y_send,
+    y_recv,
+    p_send,
+    p_recv,
+    total,
+    load_sem,
+    own_sem,
+    row_s,
+    row_r,
+    wt_s,
+    wt_r,
+    x_s,
+    x_r,
+    y_s,
+    y_r,
+    p_s,
+    p_r,
+):
+    me = lax.axis_index("ep")
+    z = me // width
+    p = me % width
+    model = normed.shape[1]
+    chunk = min(512, model)
+    loads = [
+        pltpu.make_async_copy(src, dst, load_sem.at[i])
+        for i, (src, dst) in enumerate(
+            ((sg_hbm, sg), (su_hbm, su), (sd_hbm, sd), (eg_hbm, eg), (eu_hbm, eu), (ed_hbm, ed))
+        )
+    ]
+    for load in loads:
+        load.start()
+
+    barrier = pltpu.get_barrier_semaphore()
+    for d in range(1, planes):
+        pl.semaphore_signal(
+            barrier, inc=1, device_id=(flipped(z, d) * width + p,), device_id_type=MESH
+        )
+    for r in range(1, width):
+        pl.semaphore_signal(
+            barrier, inc=1, device_id=(z * width + flipped(p, r),), device_id_type=MESH
+        )
+    pl.semaphore_wait(barrier, planes - 1 + width - 1)
+
+    sends = []
+
+    def send(src, dst, send_sem, recv_sem, target):
+        copy = pltpu.make_async_remote_copy(
+            src_ref=src,
+            dst_ref=dst,
+            send_sem=send_sem,
+            recv_sem=recv_sem,
+            device_id=(target,),
+            device_id_type=MESH,
+        )
+        copy.start()
+        sends.append(copy)
+
+    def part(buf, d, q):
+        return buf.at[d, pl.ds(pl.multiple_of(q * cap, cap), cap)]
+
+    for d in range(1, planes):
+        zt = flipped(z, d)
+        target = zt * width + p
+        send(slot_weights.at[zt], col_weights.at[d], wt_s.at[d], wt_r.at[d], target)
+        send(normed, col_rows.at[d], row_s.at[d], row_r.at[d], target)
+
+    def arrive(buf, sem):
+        pltpu.make_async_copy(buf, buf, sem).wait()
+
+    def block_weights(d):
+        return slot_weights[z] if d == 0 else col_weights[d]
+
+    def exchange(src, dst, d, send_sems, recv_sems, own):
+        for r in range(1, width):
+            q = flipped(p, r)
+            send(
+                part(src, d, q),
+                part(dst, d, p),
+                send_sems.at[d, r],
+                recv_sems.at[d, r],
+                z * width + q,
+            )
+        own_copy = pltpu.make_async_copy(part(src, d, p), part(dst, d, p), own)
+        own_copy.start()
+
+    def gathered(src, dst, d, recv_sems, own):
+        for r in range(1, width):
+            arrive(part(dst, d, flipped(p, r)), recv_sems.at[d, r])
+        pltpu.make_async_copy(part(src, d, p), part(dst, d, p), own).wait()
+
+    def dispatch(d):
+        if d:
+            arrive(col_weights.at[d], wt_r.at[d])
+            arrive(col_rows.at[d], row_r.at[d])
+        picks = jnp.where(block_weights(d).T > 0.0, 1.0, 0.0).astype(jnp.bfloat16)
+        for c in range(0, model, chunk):
+            rows = normed[:, c : c + chunk] if d == 0 else col_rows[d, :, c : c + chunk]
+            x_send[d, :, c : c + chunk] = jnp.dot(
+                picks, rows, preferred_element_type=jnp.float32
+            ).astype(jnp.bfloat16)
+        exchange(x_send, x_recv, d, x_s, x_r, own_sem.at[0, d])
+
+    def hidden(rows, w_gate, w_up):
+        gate_part = jnp.dot(rows, w_gate[...], preferred_element_type=jnp.float32)
+        up_part = jnp.dot(rows, w_up[...], preferred_element_type=jnp.float32)
+        return (jax.nn.silu(gate_part) * up_part).astype(jnp.bfloat16)
+
+    def expert(d):
+        gathered(x_send, x_recv, d, x_r, own_sem.at[0, d])
+        if d == 0:
+            for load in loads[3:]:
+                load.wait()
+        mid = hidden(x_recv[d], eg, eu)
+        for c in range(0, model, chunk):
+            y_send[d, :, c : c + chunk] = jnp.dot(
+                mid, ed[:, c : c + chunk], preferred_element_type=jnp.float32
+            ).astype(jnp.bfloat16)
+        exchange(y_send, y_recv, d, y_s, y_r, own_sem.at[1, d])
+
+    def combine(d):
+        gathered(y_send, y_recv, d, y_r, own_sem.at[1, d])
+        weights = block_weights(d)
+        high = weights.astype(jnp.bfloat16)
+        low = (weights - high.astype(jnp.float32)).astype(jnp.bfloat16)
+        for c in range(0, model, chunk):
+            rows = y_recv[d, :, c : c + chunk]
+            partial = jnp.dot(high, rows, preferred_element_type=jnp.float32) + jnp.dot(
+                low, rows, preferred_element_type=jnp.float32
+            )
+            if d == 0:
+                total[:, c : c + chunk] += partial
+            else:
+                p_send[d, :, c : c + chunk] = partial.astype(jnp.bfloat16)
+        if d:
+            send(
+                p_send.at[d], p_recv.at[d], p_s.at[d], p_r.at[d], flipped(z, d) * width + p
+            )
+
+    dispatch(0)
+    for load in loads[:3]:
+        load.wait()
+    mid = hidden(normed[...], sg, su)
+    for c in range(0, model, chunk):
+        total[:, c : c + chunk] = jnp.dot(
+            mid, sd[:, c : c + chunk], preferred_element_type=jnp.float32
+        )
+    for step in range(1, planes + 2):
+        if step < planes:
+            dispatch(step)
+        if step - 1 < planes:
+            expert(step - 1)
+        if step >= 2:
+            combine(step - 2)
+    for d in range(1, planes):
+        arrive(p_recv.at[d], p_r.at[d])
+    combined = total[...]
+    for d in range(1, planes):
+        combined = combined + p_recv[d].astype(jnp.float32)
+    out[...] = (
+        resid[...].astype(jnp.float32) + scaled_norm(combined, out_gain[...])
+    ).astype(out.dtype)
+    for copy in sends:
+        copy.wait_send()
+
+
+def moe_layer(
+    normed, resid_mid, slot_weights, moe_out_gain, experts, shared_weights, planes, width, cap
+):
+    seq_count, model = normed.shape
+    half = jnp.bfloat16
+    vmem = pl.BlockSpec(memory_space=pltpu.VMEM)
+    hbm = pl.BlockSpec(memory_space=pl.ANY)
+    slots = (planes, width * cap, model)
+    dense = (planes, seq_count, model)
+    dma = pltpu.SemaphoreType.DMA
+    weights = (*experts, *shared_weights)
+    return pl.pallas_call(
+        functools.partial(moe_kernel, planes, width, cap),
+        out_shape=jax.ShapeDtypeStruct((seq_count, model), half),
+        in_specs=[vmem] * 4 + [hbm] * 6,
+        out_specs=vmem,
+        scratch_shapes=[pltpu.VMEM(w.shape, w.dtype) for w in weights]
+        + [
+            pltpu.VMEM(dense, half),
+            pltpu.VMEM(slot_weights.shape, jnp.float32),
+            pltpu.VMEM(slots, half),
+            pltpu.VMEM(slots, half),
+            pltpu.VMEM(slots, half),
+            pltpu.VMEM(slots, half),
+            pltpu.VMEM(dense, half),
+            pltpu.VMEM(dense, half),
+            pltpu.VMEM((seq_count, model), jnp.float32),
+            dma((6,)),
+            dma((2, planes)),
+            dma((planes,)),
+            dma((planes,)),
+            dma((planes,)),
+            dma((planes,)),
+            dma((planes, width)),
+            dma((planes, width)),
+            dma((planes, width)),
+            dma((planes, width)),
+            dma((planes,)),
+            dma((planes,)),
+        ],
+        compiler_params=pltpu.CompilerParams(
+            collective_id=0, has_side_effects=True, vmem_limit_bytes=60 * 1024 * 1024
+        ),
+        name="moe_exchange",
+    )(normed, resid_mid, slot_weights, moe_out_gain[None, :], *weights)
+
+
+def slot_table(routes, route_weights, planes, width, cap):
+    seq_count, top_count = routes.shape
+    columns = planes * width * cap
+    column = jnp.arange(columns, dtype=jnp.int32)
+    column_expert = (column // cap).reshape(planes, 1, width * cap)
+    column_slot = (column % cap).reshape(planes, 1, width * cap)
+    match = routes.T[:, None, :, None] == column_expert[None]
+    chosen = jnp.any(match, axis=0)
+    weight = jnp.sum(jnp.where(match, route_weights.T[:, None, :, None], 0.0), axis=0)
+    earlier = jnp.tril(jnp.ones((seq_count, seq_count), jnp.bfloat16), -1)
+    rank = jnp.einsum(
+        "ut,ztj->zuj", earlier, chosen.astype(jnp.bfloat16), preferred_element_type=jnp.float32
+    )
+    return jnp.where(chosen & (rank == column_slot.astype(jnp.float32)), weight, 0.0)
 
 
 def state_step(
@@ -68,13 +336,6 @@
     return (activated, fresh_real.reshape(seq_count, -1), fresh_imaginary.reshape(seq_count, -1))
 
 
-def expert_rows(row_block, w_gate, w_up, w_down):
-    gate_part = jnp.dot(row_block, w_gate, preferred_element_type=jnp.float32)
-    up_part = jnp.dot(row_block, w_up, preferred_element_type=jnp.float32)
-    hidden = (jax.nn.silu(gate_part) * up_part).astype(jnp.bfloat16)
-    return jnp.dot(hidden, w_down, preferred_element_type=jnp.float32)
-
-
 def mixer_residual(residual, activated, glu_value, glu_gate, mix_gain):
     value_part = jnp.dot(activated, glu_value, preferred_element_type=jnp.float32)
     gate_part = jnp.dot(activated, glu_gate, preferred_element_type=jnp.float32)
@@ -121,47 +382,20 @@
     )
     resid_mid = mixer_residual(residual, activated, glu_value, glu_gate, mix_gain)
     normed = scaled_norm(resid_mid.astype(jnp.float32), moe_in_gain).astype(jnp.bfloat16)
-    seq_count, hidden_width = normed.shape
-    top_count = routes.shape[1]
-    expert_count = lax.axis_size("ep")
-    flat_routes = routes.reshape(-1)
-    assign_count = seq_count * top_count
-    position = jnp.arange(assign_count, dtype=jnp.int32)
-    earlier = (flat_routes[:, None] == flat_routes[None, :]) & (
-        position[None, :] < position[:, None]
-    )
-    slot_rank = jnp.sum(earlier.astype(jnp.int32), axis=1)
-    slot_index = flat_routes * capacity + slot_rank
-    slot_source = (
-        jnp.full((expert_count * capacity,), seq_count, jnp.int32)
-        .at[slot_index]
-        .set(position // top_count)
-    )
-    padded = jnp.concatenate([normed, jnp.zeros((1, hidden_width), jnp.bfloat16)], axis=0)
-    outgoing = padded[slot_source].reshape(expert_count, capacity, hidden_width)
-    received_rows = lax.all_to_all(outgoing, "ep", split_axis=0, concat_axis=0, tiled=True)
-    source_count = received_rows.shape[0]
-    item_count = received_rows.shape[1]
-    produced = expert_rows(
-        received_rows.reshape(-1, hidden_width), expert_gate[0], expert_up[0], expert_down[0]
-    ).astype(jnp.bfloat16)
-    returned = lax.all_to_all(
-        produced.reshape(source_count, item_count, hidden_width),
-        "ep",
-        split_axis=0,
-        concat_axis=0,
-        tiled=True,
-    )
-    per_assign = (
-        returned.reshape(-1, hidden_width)[slot_index]
-        .reshape(seq_count, top_count, hidden_width)
-        .astype(jnp.float32)
-    )
-    routed = jnp.sum(per_assign * route_weights[..., None], axis=1)
-    shared = expert_rows(normed, shared_gate, shared_up, shared_down)
-    combined = shared + routed
-    layer_out = (resid_mid.astype(jnp.float32) + scaled_norm(combined, moe_out_gain)).astype(
-        jnp.bfloat16
+    count = lax.axis_size("ep")
+    cap = -(-capacity // ROW_TILE) * ROW_TILE
+    planes = residual.shape[0] // cap
+    width = count // planes
+    layer_out = moe_layer(
+        normed,
+        resid_mid,
+        slot_table(routes, route_weights, planes, width, cap),
+        moe_out_gain,
+        (expert_gate[0], expert_up[0], expert_down[0]),
+        (shared_gate, shared_up, shared_down),
+        planes,
+        width,
+        cap,
     )
     return (layer_out, next_real, next_imag)
 

time: 176 us -> 109 us (0.62); the launches traced: 173 us -> 108 us
  Pallas kernels: 0 us -> 75.2 us
  blocking collectives: 53.7 us -> 0 us
  waiting for transfers between devices: 38.8 us -> 0 us
  local copies, waits for them, and re-layouts: 34.5 us -> 12.9 us
  matrix products: 32.8 us -> 15.2 us
  starting transfers between devices: 4.95 us -> 0 us
  other arithmetic: 7.54 us -> 4.01 us
    pallas_call x0 -> x1, Pallas kernels: none -> 75.2 us  [moe_layer(): pl.pallas_call(functools.partial(moe_kernel, planes, width, cap), out_sha...]
    all_to_all x1 -> x0, blocking collectives: 53.7 us -> none  [serve_rows(): lax.all_to_all(outgoing, 'ep', split_axis=0, concat_axis=0, tiled=True)]
    all_to_all x1 -> x0, waiting for transfers between devices: 38.8 us -> none  [serve_rows(): lax.all_to_all(produced.reshape(source_count, item_count, hidden_width),...]
    dot_general x4 -> x1, matrix products: 14.6 us -> 0.87 us  [slot_table(): jnp.einsum('ut,ztj->zuj', earlier, chosen.astype(jnp.bfloat16), preferred...]
    gather x2 -> x0, local copies, waits for them, and re-layouts: 10.2 us -> none  [the longest x1 6.9 us: serve_rows(): returned.reshape(-1, hidden_width)[slot_index]]
    all_to_all x1 -> x0, starting transfers between devices: 4.95 us -> none  [serve_rows(): lax.all_to_all(produced.reshape(source_count, item_count, hidden_width),...]
    unnamed x47 -> x38, local copies, waits for them, and re-layouts: 16.2 us -> 12 us
    convert_element_type x1 -> x0, local copies, waits for them, and re-layouts: 3.89 us -> none  [serve_rows(): per_assign = returned.reshape(-1, hidden_width)[slot_index].reshape(seq_c...]
  transfers between devices with their start and end apart: 1 -> 0, of which waited for: 1 -> 0; matrix products, arithmetic and copies ran while one was open for 5% -> 0% of each run, Pallas kernels for 0% -> 0%
where the time goes in v1:
time: 109 us; the launch traced here: 108 us
  Pallas kernels  75.2 us (69%)
  matrix products  15.2 us (14%)
  local copies, waits for them, and re-layouts  12.9 us (12%)
  other arithmetic  4.01 us (4%)
    pallas_call x1, Pallas kernels, moe_layer(): pl.pallas_call(functools.partial(moe_kernel, planes, width, cap), out_sha...  75.2 us
    unnamed x38, local copies, waits for them, and re-layouts  12 us
    dot_general x1, matrix products, state_step(): jnp.einsum('tgc,gpc->tgp', feed_rows, bbar_im, precision=lax.Precision.HI...  4.69 us
    dot_general x1, matrix products, state_step(): jnp.einsum('tgc,gpc->tgp', feed_rows, bbar_re, precision=lax.Precision.HI...  3.24 us
    dot_general x1, matrix products, mixer_residual(): gate_part = jnp.dot(activated, glu_gate, preferred_element_type=jnp.float32)  3.22 us

profile of v1, /device:TPU:17, one launch (start us, length us, event | category | flops | bytes accessed | tf_op | source)
XLA Modules:
  0.0 108.2 jit_solution(11136455298517268909)
XLA Ops:
  0.6 0.0 copy-start
  0.6 0.7 exp.9
  1.4 0.9 compare_reduce_fusion
  2.2 0.9 fusion.6
  3.1 0.9 fusion.5.slot_weights
  4.0 1.0 add_divide_fusion
  5.0 1.1 copy.47
  6.1 1.8 %copy.45 = f32[64,4096]{0,1:T(8,128)S(1)} copy(f32[64,4096]{1,0:T(8,128)} %param.27) | data formatting | bytes 2097152 | tf_op args[2]
  7.9 0.0 copy-start.7
  7.9 0.0 copy-start.8
  7.9 3.2 %copy.46 = f32[64,4096]{0,1:T(8,128)} copy(f32[64,4096]{1,0:T(8,128)} %param.28) | data formatting | bytes 2097152 | tf_op args[3]
  11.2 0.0 copy-done.7
  11.2 0.0 copy-done.8
  11.2 0.0 copy-start.1
  11.2 4.7 %bitcast_add_fusion = f32[64,64,64]{0,2,1:T(8,128)S(1)} fusion(f32[64,64,64]{0,2,1:T(8,128)S(1)} %bitcast.38, f32[64,64,64]{0,2,1:T(8,128)} %bitcast.40, bf16[64,64,16]{0,2,1:T(8,128)(2,1)S(1)} %bitcast.44, f32[64,64]{1,0:T(8,128)S(1)} %get-tuple-element.17, f32[64,64]{1,0:T(8,128)S(1)} %get-tuple-element.15, bf16[64,64,16]{1,2,0:T(8,128)(2,1)S(1)} %copy-done.7, ...), kind=kOutput, calls=%fused_computation.5 | convolution fusion | flops 51707904 | bytes 3604480 | tf_op jit(solution)/shard_map/tgc,gpc->tgp/dot_general | solution.py:316
  15.9 0.0 copy-done.1
  15.9 0.0 copy-start.4
  15.9 3.2 %bitcast_add_fusion.1 = f32[64,64,64]{0,2,1:T(8,128)S(1)} fusion(f32[64,64,64]{0,2,1:T(8,128)S(1)} %bitcast.41, f32[64,64,64]{0,2,1:T(8,128)S(1)} %bitcast.39, bf16[64,64,16]{0,2,1:T(8,128)(2,1)S(1)} %bitcast.45, f32[64,64]{1,0:T(8,128)S(1)} %get-tuple-element.17, f32[64,64]{1,0:T(8,128)S(1)} %get-tuple-element.15, bf16[64,64,16]{1,2,0:T(8,128)(2,1)S(1)} %copy-done.7, ...), kind=kOutput, calls=%fused_computation.6 | convolution fusion | flops 51707904 | bytes 3604480 | tf_op jit(solution)/shard_map/tgc,gpc->tgp/dot_general | solution.py:315
  19.2 0.0 copy-start.2
  19.2 0.0 copy-start.12
  19.2 0.0 copy-done
  19.2 1.1 %fusion.38 = f32[64,64,16]{1,2,0:T(8,128)S(1)} fusion(f32[64,64,64]{0,2,1:T(8,128)S(1)} %bitcast_add_fusion.1, bf16[64,16,64]{2,1,0:T(8,128)(2,1)S(1)} %copy-done), kind=kOutput, calls=%fused_computation.69 | convolution fusion | flops 50331648 | bytes 1441792 | tf_op jit(solution)/shard_map/ukb,krb->ukr/dot_general | solution.py:321
  20.3 0.0 copy-done.4
  20.3 0.0 copy-done.12
  20.3 0.0 copy-start.15
  20.3 1.1 %convolution_subtract_fusion = f32[64,64,16]{1,2,0:T(8,128)S(1)} fusion(f32[64,64,16]{1,2,0:T(8,128)S(1)} %fusion.38, f32[64,64,64]{0,2,1:T(8,128)S(1)} %bitcast_add_fusion, bf16[64,16,64]{2,1,0:T(8,128)(2,1)S(1)} %copy-done.12), kind=kOutput, calls=%fused_computation.7 | convolution fusion | flops 50397184 | bytes 1703936 | tf_op jit(solution)/shard_map/ukb,krb->ukr/dot_general | solution.py:326
  21.4 0.0 copy-done.2
  21.5 0.2 copy.50
  21.6 0.0 copy-done.10
  21.7 0.0 copy-done.15
  21.7 0.1 fusion.21
  21.8 0.0 copy-start.5
  21.8 3.2 %fusion.2 = f32[64,2048]{1,0:T(8,128)S(1)} fusion(bf16[64,1024]{1,0:T(8,128)(2,1)S(1)} %fusion.21, bf16[1024,2048]{1,0:T(8,128)(2,1)} %param.38), kind=kOutput, calls=%fused_computation.4 | convolution fusion | flops 268828672 | bytes 4849664 | tf_op jit(solution)/shard_map/dot_general | solution.py:341
  25.0 0.2 copy-done.5
  25.2 1.0 multiply_reduce_fusion
  26.2 0.0 copy-done.11
  26.2 0.0 copy-done.13
  26.2 0.3 fusion.11
  26.5 0.0 copy-done.14
  26.5 0.8 fusion.13.normed
  27.4 0.0 copy-done.6
  27.4 75.2 %moe_exchange.1 = bf16[64,2048]{1,0:T(8,128)(2,1)} custom-call(bf16[64,2048]{1,0:T(8,128)(2,1)} %fusion.13.normed, bf16[64,2048]{1,0:T(8,128)(2,1)} %copy-done.6, f32[4,64,128]{2,1,0:T(8,128)} %fusion.5.slot_weights, f32[1,2048]{1,0:T(1,128)} %bitcast.52, bf16[2048,512]{1,0:T(8,128)(2,1)} %bitcast.47, bf16[2048,512]{1,0:T(8,128)(2,1)} %bitcast.48, ...), custom_call_target="tpu_custom_call" | custom-call | tf_op jit(solution)/shard_map/moe_exchange/pallas_call | solution.py:233
  102.6 0.0 copy-start.3
  102.6 3.3 %copy.52 = f32[64,4096]{1,0:T(8,128)} copy(f32[64,4096]{0,1:T(8,128)} %bitcast.43) | data formatting | bytes 2097152
  105.9 0.0 copy-done.3
  105.9 1.6 %copy.51 = f32[64,4096]{1,0:T(8,128)} copy(f32[64,4096]{0,1:T(8,128)S(1)} %bitcast.42) | data formatting | bytes 2097152
  107.5 0.0 copy-done.9
  107.5 0.7 copy.56
  (11 shorter events, 0.1 us)
Async XLA Ops:
  0.6 18.6 %copy-start = (bf16[64,16,64]{2,1,0:T(8,128)(2,1)S(1)}, bf16[64,16,64]{2,1,0:T(8,128)(2,1)}, u32[]{:S(2)}) copy-start(bf16[64,16,64]{2,1,0:T(8,128)(2,1)} %param.34) | copy-start | bytes 393220
  7.9 3.3 %copy-start.7 = (bf16[64,64,16]{1,2,0:T(8,128)(2,1)S(1)}, bf16[64,64,16]{1,2,0:T(8,128)(2,1)}, u32[]{:S(2)}) copy-start(bf16[64,64,16]{1,2,0:T(8,128)(2,1)} %param.32) | copy-start | bytes 393220
  7.9 3.3 %copy-start.8 = (bf16[64,64,16]{1,2,0:T(8,128)(2,1)S(1)}, bf16[64,64,16]{1,2,0:T(8,128)(2,1)}, u32[]{:S(2)}) copy-start(bf16[64,64,16]{1,2,0:T(8,128)(2,1)} %param.33) | copy-start | bytes 393220
  11.2 4.7 %copy-start.1 = (f32[64,4096]{0,1:T(8,128)S(1)}, f32[64,4096]{0,1:T(8,128)}, u32[]{:S(2)}) copy-start(f32[64,4096]{0,1:T(8,128)} %copy.46) | copy-start | bytes 3145732
  15.9 4.4 %copy-start.4 = (f32[64,64,64]{0,2,1:T(8,128)}, f32[64,64,64]{0,2,1:T(8,128)S(1)}, u32[]{:S(2)}) copy-start(f32[64,64,64]{0,2,1:T(8,128)S(1)} %bitcast_add_fusion) | copy-start | bytes 3145732
  19.2 2.3 %copy-start.2 = (f32[64,64,64]{0,2,1:T(8,128)}, f32[64,64,64]{0,2,1:T(8,128)S(1)}, u32[]{:S(2)}) copy-start(f32[64,64,64]{0,2,1:T(8,128)S(1)} %bitcast_add_fusion.1) | copy-start | bytes 3145732
  19.2 1.1 %copy-start.12 = (bf16[64,16,64]{2,1,0:T(8,128)(2,1)S(1)}, bf16[64,16,64]{2,1,0:T(8,128)(2,1)}, u32[]{:S(2)}) copy-start(bf16[64,16,64]{2,1,0:T(8,128)(2,1)} %param.35) | copy-start | bytes 393220
  20.3 1.3 %copy-start.10 = (bf16[64,1024]{1,0:T(8,128)(2,1)S(1)}, bf16[64,1024]{1,0:T(8,128)(2,1)}, u32[]{:S(2)}) copy-start(bf16[64,1024]{1,0:T(8,128)(2,1)} %param.26) | copy-start | bytes 393220
  20.3 1.3 %copy-start.15 = (f32[1024]{0:T(1024)S(1)}, f32[1024]{0:T(1024)}, u32[]{:S(2)}) copy-start(f32[1024]{0:T(1024)} %param.36) | copy-start | bytes 12292
  21.8 3.5 %copy-start.5 = (bf16[1024,2048]{1,0:T(8,128)(2,1)S(1)}, bf16[1024,2048]{1,0:T(8,128)(2,1)}, u32[]{:S(2)}) copy-start(bf16[1024,2048]{1,0:T(8,128)(2,1)} %param.37) | copy-start | bytes 12582916
  25.2 1.0 copy-start.11
  25.2 1.0 copy-start.13
  25.2 1.3 %copy-start.14 = (f32[2048]{0:T(1024)S(1)}, f32[2048]{0:T(1024)}, u32[]{:S(2)}) copy-start(f32[2048]{0:T(1024)} %param.40) | copy-start | bytes 24580
  26.5 0.9 copy-start.6
  102.6 3.3 %copy-start.3 = (f32[64,64,64]{0,2,1:T(8,128)S(1)}, f32[64,64,64]{0,2,1:T(8,128)}, u32[]{:S(2)}) copy-start(f32[64,64,64]{0,2,1:T(8,128)} %copy-done.2) | copy-start | bytes 3145732
  105.9 1.6 %copy-start.9 = (bf16[64,2048]{1,0:T(8,128)(2,1)S(1)}, bf16[64,2048]{1,0:T(8,128)(2,1)}, u32[]{:S(2)}) copy-start(bf16[64,2048]{1,0:T(8,128)(2,1)} %moe_exchange.1) | copy-start | bytes 786436

commit v2 on v1

--- a/solution.py
+++ b/solution.py
@@ -9,6 +9,7 @@
 
 norm_eps = 1e-06
 ROW_TILE = 16
+PIECES = 2
 MESH = pl.DeviceIdType.MESH
 
 
@@ -76,7 +77,8 @@
     z = me // width
     p = me % width
     model = normed.shape[1]
-    chunk = min(512, model)
+    chunk = model // PIECES
+    columns = [slice(i * chunk, (i + 1) * chunk) for i in range(PIECES)]
     loads = [
         pltpu.make_async_copy(src, dst, load_sem.at[i])
         for i, (src, dst) in enumerate(
@@ -111,14 +113,21 @@
         copy.start()
         sends.append(copy)
 
-    def part(buf, d, q):
-        return buf.at[d, pl.ds(pl.multiple_of(q * cap, cap), cap)]
+    def part(buf, d, q, i):
+        return buf.at[d, pl.ds(pl.multiple_of(q * cap, cap), cap), columns[i]]
 
     for d in range(1, planes):
         zt = flipped(z, d)
         target = zt * width + p
         send(slot_weights.at[zt], col_weights.at[d], wt_s.at[d], wt_r.at[d], target)
-        send(normed, col_rows.at[d], row_s.at[d], row_r.at[d], target)
+        for i in range(PIECES):
+            send(
+                normed.at[:, columns[i]],
+                col_rows.at[d, :, columns[i]],
+                row_s.at[d, i],
+                row_r.at[d, i],
+                target,
+            )
 
     def arrive(buf, sem):
         pltpu.make_async_copy(buf, buf, sem).wait()
@@ -126,35 +135,34 @@
     def block_weights(d):
         return slot_weights[z] if d == 0 else col_weights[d]
 
-    def exchange(src, dst, d, send_sems, recv_sems, own):
+    def exchange(src, dst, d, i, send_sems, recv_sems, own):
         for r in range(1, width):
             q = flipped(p, r)
             send(
-                part(src, d, q),
-                part(dst, d, p),
-                send_sems.at[d, r],
-                recv_sems.at[d, r],
+                part(src, d, q, i),
+                part(dst, d, p, i),
+                send_sems.at[d, r, i],
+                recv_sems.at[d, r, i],
                 z * width + q,
             )
-        own_copy = pltpu.make_async_copy(part(src, d, p), part(dst, d, p), own)
-        own_copy.start()
-
-    def gathered(src, dst, d, recv_sems, own):
+        pltpu.make_async_copy(part(src, d, p, i), part(dst, d, p, i), own).start()
+
+    def gathered(src, dst, d, i, recv_sems, own):
         for r in range(1, width):
-            arrive(part(dst, d, flipped(p, r)), recv_sems.at[d, r])
-        pltpu.make_async_copy(part(src, d, p), part(dst, d, p), own).wait()
-
-    def dispatch(d):
+            arrive(part(dst, d, flipped(p, r), i), recv_sems.at[d, r, i])
+        pltpu.make_async_copy(part(src, d, p, i), part(dst, d, p, i), own).wait()
+
+    def dispatch(d, i):
         if d:
-            arrive(col_weights.at[d], wt_r.at[d])
-            arrive(col_rows.at[d], row_r.at[d])
+            if i == 0:
+                arrive(col_weights.at[d], wt_r.at[d])
+            arrive(col_rows.at[d, :, columns[i]], row_r.at[d, i])
         picks = jnp.where(block_weights(d).T > 0.0, 1.0, 0.0).astype(jnp.bfloat16)
-        for c in range(0, model, chunk):
-            rows = normed[:, c : c + chunk] if d == 0 else col_rows[d, :, c : c + chunk]
-            x_send[d, :, c : c + chunk] = jnp.dot(
-                picks, rows, preferred_element_type=jnp.float32
-            ).astype(jnp.bfloat16)
-        exchange(x_send, x_recv, d, x_s, x_r, own_sem.at[0, d])
+        rows = normed[:, columns[i]] if d == 0 else col_rows[d, :, columns[i]]
+        x_send[d, :, columns[i]] = jnp.dot(
+            picks, rows, preferred_element_type=jnp.float32
+        ).astype(jnp.bfloat16)
+        exchange(x_send, x_recv, d, i, x_s, x_r, own_sem.at[0, d, i])
 
     def hidden(rows, w_gate, w_up):
         gate_part = jnp.dot(rows, w_gate[...], preferred_element_type=jnp.float32)
@@ -162,53 +170,71 @@
         return (jax.nn.silu(gate_part) * up_part).astype(jnp.bfloat16)
 
     def expert(d):
-        gathered(x_send, x_recv, d, x_r, own_sem.at[0, d])
+        for i in range(PIECES):
+            gathered(x_send, x_recv, d, i, x_r, own_sem.at[0, d, i])
         if d == 0:
             for load in loads[3:]:
                 load.wait()
         mid = hidden(x_recv[d], eg, eu)
-        for c in range(0, model, chunk):
-            y_send[d, :, c : c + chunk] = jnp.dot(
-                mid, ed[:, c : c + chunk], preferred_element_type=jnp.float32
+        for i in range(PIECES):
+            y_send[d, :, columns[i]] = jnp.dot(
+                mid, ed[:, columns[i]], preferred_element_type=jnp.float32
             ).astype(jnp.bfloat16)
-        exchange(y_send, y_recv, d, y_s, y_r, own_sem.at[1, d])
+            exchange(y_send, y_recv, d, i, y_s, y_r, own_sem.at[1, d, i])
 
     def combine(d):
-        gathered(y_send, y_recv, d, y_r, own_sem.at[1, d])
         weights = block_weights(d)
         high = weights.astype(jnp.bfloat16)
         low = (weights - high.astype(jnp.float32)).astype(jnp.bfloat16)
-        for c in range(0, model, chunk):
-            rows = y_recv[d, :, c : c + chunk]
+        for i in range(PIECES):
+            gathered(y_send, y_recv, d, i, y_r, own_sem.at[1, d, i])
+            rows = y_recv[d, :, columns[i]]
             partial = jnp.dot(high, rows, preferred_element_type=jnp.float32) + jnp.dot(
                 low, rows, preferred_element_type=jnp.float32
             )
             if d == 0:
-                total[:, c : c + chunk] += partial
+                total[:, columns[i]] += partial
             else:
-                p_send[d, :, c : c + chunk] = partial.astype(jnp.bfloat16)
-        if d:
-            send(
-                p_send.at[d], p_recv.at[d], p_s.at[d], p_r.at[d], flipped(z, d) * width + p
-            )
-
-    dispatch(0)
+                p_send[d, :, columns[i]] = partial.astype(jnp.bfloat16)
+                send(
+                    p_send.at[d, :, columns[i]],
+                    p_recv.at[d, :, columns[i]],
+                    p_s.at[d, i],
+                    p_r.at[d, i],
+                    flipped(z, d) * width + p,
+                )
+
+    for i in range(PIECES):
+        dispatch(0, i)
     for load in loads[:3]:
         load.wait()
     mid = hidden(normed[...], sg, su)
-    for c in range(0, model, chunk):
-        total[:, c : c + chunk] = jnp.dot(
-            mid, sd[:, c : c + chunk], preferred_element_type=jnp.float32
+    for i in range(PIECES):
+        total[:, columns[i]] = jnp.dot(
+            mid, sd[:, columns[i]], preferred_element_type=jnp.float32
         )
-    for step in range(1, planes + 2):
-        if step < planes:
-            dispatch(step)
-        if step - 1 < planes:
-            expert(step - 1)
-        if step >= 2:
-            combine(step - 2)
+    last = planes - 1
     for d in range(1, planes):
-        arrive(p_recv.at[d], p_r.at[d])
+        for i in range(PIECES):
+            dispatch(d, i)
+            if i == 0 and d > 1 and d < last:
+                expert(d - 1)
+        if d == 1:
+            expert(0)
+    if last > 1:
+        expert(last - 1)
+    for d in range(1, last - 1):
+        combine(d)
+    if last > 0:
+        expert(last)
+    if last > 1:
+        combine(last - 1)
+    combine(0)
+    if last > 0:
+        combine(last)
+    for d in range(1, planes):
+        for i in range(PIECES):
+            arrive(p_recv.at[d, :, columns[i]], p_r.at[d, i])
     combined = total[...]
     for d in range(1, planes):
         combined = combined + p_recv[d].astype(jnp.float32)
@@ -247,17 +273,14 @@
             pltpu.VMEM(dense, half),
             pltpu.VMEM((seq_count, model), jnp.float32),
             dma((6,)),
-            dma((2, planes)),
+            dma((2, planes, PIECES)),
+            dma((planes, PIECES)),
+            dma((planes, PIECES)),
             dma((planes,)),
             dma((planes,)),
-            dma((planes,)),
-            dma((planes,)),
-            dma((planes, width)),
-            dma((planes, width)),
-            dma((planes, width)),
-            dma((planes, width)),
-            dma((planes,)),
-            dma((planes,)),
+            *[dma((planes, width, PIECES))] * 4,
+            dma((planes, PIECES)),
+            dma((planes, PIECES)),
         ],
         compiler_params=pltpu.CompilerParams(
             collective_id=0, has_side_effects=True, vmem_limit_bytes=60 * 1024 * 1024
@@ -282,7 +305,137 @@
     return jnp.where(chosen & (rank == column_slot.astype(jnp.float32)), weight, 0.0)
 
 
-def state_step(
+def wide(block, groups):
+    rows, states = block.shape
+    tiled = jnp.concatenate([block] * groups, axis=1)
+    shape = (rows, groups * states)
+    row = lax.broadcasted_iota(jnp.int32, shape, 0) // (rows // groups)
+    column = lax.broadcasted_iota(jnp.int32, shape, 1) // states
+    return jnp.where(row == column, tiled, 0.0)
+
+
+def halves(value):
+    high = value.astype(jnp.bfloat16)
+    return high, (value - high.astype(jnp.float32)).astype(jnp.bfloat16)
+
+
+def mixer_kernel(
+    groups,
+    residual,
+    feed,
+    state_re,
+    state_im,
+    abar_re,
+    abar_im,
+    bbar_re,
+    bbar_im,
+    out_re,
+    out_im,
+    skip,
+    value_hbm,
+    gate_hbm,
+    mix_gain,
+    in_gain,
+    resid_mid,
+    normed,
+    next_re,
+    next_im,
+    old_re,
+    old_im,
+    new_re,
+    new_im,
+    value,
+    gate,
+    active,
+    in_sem,
+    out_sem,
+    glu_sem,
+):
+    states = abar_re.shape[1]
+    chans = bbar_re.shape[0] // abar_re.shape[0]
+    lanes = groups * states
+    feeds = groups * chans
+    count = abar_re.shape[0] // groups
+
+    def piece(n):
+        return slice(n * lanes, (n + 1) * lanes)
+
+    def read(n):
+        return [
+            pltpu.make_async_copy(src.at[:, piece(n)], dst.at[:, piece(n)], in_sem.at[k, n])
+            for k, (src, dst) in enumerate(((state_re, old_re), (state_im, old_im)))
+        ]
+
+    def write(n):
+        return [
+            pltpu.make_async_copy(src.at[:, piece(n)], dst.at[:, piece(n)], out_sem.at[k, n])
+            for k, (src, dst) in enumerate(((new_re, next_re), (new_im, next_im)))
+        ]
+
+    glu = [
+        pltpu.make_async_copy(value_hbm, value, glu_sem.at[0]),
+        pltpu.make_async_copy(gate_hbm, gate, glu_sem.at[1]),
+    ]
+    for n in range(count):
+        for copy in read(n):
+            copy.start()
+    for copy in glu:
+        copy.start()
+
+    nt = (((1,), (1,)), ((), ()))
+    for n in range(count):
+        rows = slice(n * feeds, (n + 1) * feeds)
+        some = slice(n * groups, (n + 1) * groups)
+        u = feed[:, rows]
+        a_re = jnp.sum(wide(abar_re[some, :], groups), axis=0, keepdims=True)
+        a_im = jnp.sum(wide(abar_im[some, :], groups), axis=0, keepdims=True)
+
+        def force(bbar):
+            high, low = halves(wide(bbar[rows, :], groups))
+            return jnp.dot(u, high, preferred_element_type=jnp.float32) + jnp.dot(
+                u, low, preferred_element_type=jnp.float32
+            )
+
+        def readout(fresh, matrix):
+            weights = wide(matrix[rows, :].astype(jnp.float32), groups).astype(jnp.bfloat16)
+            high, low = halves(fresh)
+            return lax.dot_general(
+                high, weights, nt, preferred_element_type=jnp.float32
+            ) + lax.dot_general(low, weights, nt, preferred_element_type=jnp.float32)
+
+        for copy in read(n):
+            copy.wait()
+        was_re, was_im = old_re[:, piece(n)], old_im[:, piece(n)]
+        fresh_re = a_re * was_re - a_im * was_im + force(bbar_re)
+        fresh_im = a_re * was_im + a_im * was_re + force(bbar_im)
+        new_re[:, piece(n)] = fresh_re
+        new_im[:, piece(n)] = fresh_im
+        for copy in write(n):
+            copy.start()
+        mixed = (
+            readout(fresh_re, out_re)
+            - readout(fresh_im, out_im)
+            + skip[:, rows] * u.astype(jnp.float32)
+        )
+        active[:, rows] = jax.nn.gelu(mixed).astype(jnp.bfloat16)
+    for copy in glu:
+        copy.wait()
+    acts = active[...]
+    value_part = jnp.dot(acts, value[...], preferred_element_type=jnp.float32)
+    gate_part = jnp.dot(acts, gate[...], preferred_element_type=jnp.float32)
+    branch = value_part * jax.nn.sigmoid(gate_part)
+    mid = (residual[...].astype(jnp.float32) + scaled_norm(branch, mix_gain[...])).astype(
+        jnp.bfloat16
+    )
+    resid_mid[...] = mid
+    normed[...] = scaled_norm(mid.astype(jnp.float32), in_gain[...]).astype(jnp.bfloat16)
+    for n in range(count):
+        for copy in write(n):
+            copy.wait()
+
+
+def mixer(
+    residual,
     branch_in,
     state_real,
     state_imag,
@@ -294,10 +447,12 @@
     output_matrix_real,
     output_matrix_imaginary,
     skip_gain,
+    glu_value,
+    glu_gate,
+    mix_gain,
+    moe_in_gain,
 ):
-    seq_count = branch_in.shape[0]
     group_count, state_count = decay_rate.shape
-    chan_count = input_real.shape[2]
     step_size = jnp.exp(log_step)[:, None]
     magnitude = jnp.exp(-decay_rate * step_size)
     abar_re = magnitude * jnp.cos(frequency * step_size)
@@ -305,42 +460,57 @@
     lam_re = -decay_rate
     denominator = lam_re * lam_re + frequency * frequency
     numer_re = abar_re - 1.0
-    coef_re = (numer_re * lam_re + abar_im * frequency) / denominator
-    coef_im = (abar_im * lam_re - numer_re * frequency) / denominator
-    b_real = input_real.astype(jnp.float32)
-    b_imag = input_imag.astype(jnp.float32)
-    bbar_re = coef_re[..., None] * b_real - coef_im[..., None] * b_imag
-    bbar_im = coef_re[..., None] * b_imag + coef_im[..., None] * b_real
-    feed_rows = branch_in.astype(jnp.float32).reshape(seq_count, group_count, chan_count)
-    forcing_real = jnp.einsum("tgc,gpc->tgp", feed_rows, bbar_re, precision=lax.Precision.HIGHEST)
-    drive_im = jnp.einsum("tgc,gpc->tgp", feed_rows, bbar_im, precision=lax.Precision.HIGHEST)
-    old_re = state_real.reshape(seq_count, group_count, state_count)
-    old_im = state_imag.reshape(seq_count, group_count, state_count)
-    fresh_real = abar_re * old_re - abar_im * old_im + forcing_real
-    fresh_imaginary = abar_re * old_im + abar_im * old_re + drive_im
-    state_readout = jnp.einsum(
-        "ukb,krb->ukr",
-        fresh_real,
-        output_matrix_real.astype(jnp.float32),
-        precision=lax.Precision.HIGHEST,
-    ) - jnp.einsum(
-        "ukb,krb->ukr",
-        fresh_imaginary,
-        output_matrix_imaginary.astype(jnp.float32),
-        precision=lax.Precision.HIGHEST,
-    )
-    mixed_rows = state_readout.reshape(
-        seq_count, group_count * chan_count
-    ) + skip_gain * branch_in.astype(jnp.float32)
-    activated = jax.nn.gelu(mixed_rows).astype(jnp.bfloat16)
-    return (activated, fresh_real.reshape(seq_count, -1), fresh_imaginary.reshape(seq_count, -1))
-
-
-def mixer_residual(residual, activated, glu_value, glu_gate, mix_gain):
-    value_part = jnp.dot(activated, glu_value, preferred_element_type=jnp.float32)
-    gate_part = jnp.dot(activated, glu_gate, preferred_element_type=jnp.float32)
-    branch = value_part * jax.nn.sigmoid(gate_part)
-    return (residual.astype(jnp.float32) + scaled_norm(branch, mix_gain)).astype(jnp.bfloat16)
+    coef_re = ((numer_re * lam_re + abar_im * frequency) / denominator)[:, None, :]
+    coef_im = ((abar_im * lam_re - numer_re * frequency) / denominator)[:, None, :]
+    b_real = input_real.astype(jnp.float32).transpose(0, 2, 1)
+    b_imag = input_imag.astype(jnp.float32).transpose(0, 2, 1)
+    bbar_re = (coef_re * b_real - coef_im * b_imag).reshape(-1, state_count)
+    bbar_im = (coef_re * b_imag + coef_im * b_real).reshape(-1, state_count)
+    groups = max(1, 128 // input_real.shape[2])
+    count = group_count // groups
+    vmem = pl.BlockSpec(memory_space=pltpu.VMEM)
+    hbm = pl.BlockSpec(memory_space=pl.ANY)
+    state = state_real.shape
+    rows = jax.ShapeDtypeStruct(residual.shape, jnp.bfloat16)
+    dma = pltpu.SemaphoreType.DMA
+    return pl.pallas_call(
+        functools.partial(mixer_kernel, groups),
+        out_shape=(
+            rows,
+            rows,
+            jax.ShapeDtypeStruct(state, jnp.float32),
+            jax.ShapeDtypeStruct(state, jnp.float32),
+        ),
+        in_specs=[vmem, vmem, hbm, hbm] + [vmem] * 7 + [hbm, hbm, vmem, vmem],
+        out_specs=(vmem, vmem, hbm, hbm),
+        scratch_shapes=[
+            *[pltpu.VMEM(state, jnp.float32)] * 4,
+            pltpu.VMEM(glu_value.shape, jnp.bfloat16),
+            pltpu.VMEM(glu_gate.shape, jnp.bfloat16),
+            pltpu.VMEM(branch_in.shape, jnp.bfloat16),
+            dma((2, count)),
+            dma((2, count)),
+            dma((2,)),
+        ],
+        compiler_params=pltpu.CompilerParams(vmem_limit_bytes=60 * 1024 * 1024),
+        name="mixer",
+    )(
+        residual,
+        branch_in,
+        state_real,
+        state_imag,
+        abar_re,
+        abar_im,
+        bbar_re,
+        bbar_im,
+        output_matrix_real.reshape(-1, state_count),
+        output_matrix_imaginary.reshape(-1, state_count),
+        skip_gain[None, :],
+        glu_value,
+        glu_gate,
+        mix_gain[None, :],
+        moe_in_gain[None, :],
+    )
 
 
 def serve_rows(
@@ -367,7 +537,8 @@
         shared_up,
         shared_down,
     ) = params
-    activated, next_real, next_imag = state_step(
+    resid_mid, normed, next_real, next_imag = mixer(
+        residual,
         branch_in,
         state_real,
         state_imag,
@@ -379,9 +550,11 @@
         output_matrix_real,
         output_matrix_imaginary,
         skip_gain,
-    )
-    resid_mid = mixer_residual(residual, activated, glu_value, glu_gate, mix_gain)
-    normed = scaled_norm(resid_mid.astype(jnp.float32), moe_in_gain).astype(jnp.bfloat16)
+        glu_value,
+        glu_gate,
+        mix_gain,
+        moe_in_gain,
+    )
     count = lax.axis_size("ep")
     cap = -(-capacity // ROW_TILE) * ROW_TILE
     planes = residual.shape[0] // cap

time: 109 us -> 92.5 us (0.85)
  matrix products: 15.2 us -> 0.88 us
  local copies, waits for them, and re-layouts: 12.9 us -> 2.34 us
  Pallas kernels: 75.2 us -> 84.2 us
    dot_general x6 -> x0, matrix products: 14.3 us -> none  [the longest x1 4.69 us: state_step(): jnp.einsum('tgc,gpc->tgp', feed_rows, bbar_im, precision=lax.Precision.HI...]
    unnamed x38 -> x5, local copies, waits for them, and re-layouts: 12 us -> 1.68 us
    pallas_call x0 -> x1, Pallas kernels: none -> 10.2 us  [mixer(): pl.pallas_call(functools.partial(mixer_kernel, groups), out_shape=(rows,...]
    add x0 -> x1, other arithmetic: none -> 2.16 us  [mixer(): bbar_im = (coef_re * b_imag + coef_im * b_real).reshape(-1, state_count)]
    pallas_call x1, Pallas kernels: 75.2 us -> 74 us  [moe_layer(): pl.pallas_call(functools.partial(moe_kernel, planes, width, cap), out_sha...]
where the time goes in v2:
time: 92.5 us; the launch traced here: 92.2 us
  Pallas kernels  84.2 us (91%)
  other arithmetic  4.13 us (4%)
  local copies, waits for them, and re-layouts  2.34 us (3%)
    pallas_call x1, Pallas kernels, moe_layer(): pl.pallas_call(functools.partial(moe_kernel, planes, width, cap), out_sha...  74 us
    pallas_call x1, Pallas kernels, mixer(): pl.pallas_call(functools.partial(mixer_kernel, groups), out_shape=(rows,...  10.2 us
    add x1, other arithmetic, mixer(): bbar_im = (coef_re * b_imag + coef_im * b_real).reshape(-1, state_count)  2.16 us

profile of v2, /device:TPU:17, one launch (start us, length us, event | category | flops | bytes accessed | tf_op | source)
XLA Modules:
  0.0 92.2 jit_solution(7846614267290480310)
XLA Ops:
  0.6 0.7 exp.6
  1.3 1.6 %add_divide_fusion = (f32[64,64]{1,0:T(8,128)S(1)}, f32[64,64]{1,0:T(8,128)}, f32[64,64]{1,0:T(8,128)S(1)}, f32[64,64]{1,0:T(8,128)}) fusion(f32[64,64]{1,0:T(8,128)} %param.30, f32[64,64]{1,0:T(8,128)} %param.29, f32[64]{0:T(128)S(1)} %exp.6), kind=kLoop, calls=%fused_computation.16 | loop fusion | flops 69632 | bytes 98560 | tf_op jit(solution)/shard_map/div | solution.py:463
  2.9 2.2 %fusion.5 = (f32[64,64,16]{1,2,0:T(8,128)}, f32[64,64,16]{1,2,0:T(8,128)}) fusion(bf16[64,64,16]{1,2,0:T(8,128)(2,1)} %param.32, bf16[64,64,16]{1,2,0:T(8,128)(2,1)} %param.33, f32[64,64]{1,0:T(8,128)S(1)} %get-tuple-element.15, f32[64,64]{1,0:T(8,128)S(1)} %get-tuple-element.13), kind=kLoop, calls=%fused_computation.12 | loop fusion | flops 524288 | bytes 819200 | tf_op jit(solution)/shard_map/add | solution.py:468
  5.1 0.0 copy-start
  5.1 0.0 copy-start.1
  5.1 10.2 %mixer.1 = (bf16[64,2048]{1,0:T(8,128)(2,1)}, bf16[64,2048]{1,0:T(8,128)(2,1)}, f32[64,4096]{1,0:T(8,128)}, f32[64,4096]{1,0:T(8,128)}) custom-call(bf16[64,2048]{1,0:T(8,128)(2,1)} %residual.1, bf16[64,1024]{1,0:T(8,128)(2,1)} %feed.1, f32[64,4096]{1,0:T(8,128)} %state_re.1, f32[64,4096]{1,0:T(8,128)} %state_im.1, f32[64,64]{1,0:T(8,128)} %get-tuple-element.14.abar_re, ...), custom_call_target="tpu_custom_call" | custom-call | tf_op jit(solution)/shard_map/mixer/pallas_call | solution.py:476
  15.3 0.0 copy-done
  15.3 0.0 copy-done.1
  15.3 0.2 fusion.3
  15.5 0.2 compare_reduce_fusion
  15.7 0.9 fusion.2.slot_weights
  16.5 74.0 %moe_exchange.1 = bf16[64,2048]{1,0:T(8,128)(2,1)} custom-call(bf16[64,2048]{1,0:T(8,128)(2,1)} %get-tuple-element.7.normed, bf16[64,2048]{1,0:T(8,128)(2,1)} %get-tuple-element.8.resid, f32[4,64,128]{2,1,0:T(8,128)} %fusion.2.slot_weights, f32[1,2048]{1,0:T(1,128)} %bitcast.38, bf16[2048,512]{1,0:T(8,128)(2,1)} %bitcast.29, bf16[2048,512]{1,0:T(8,128)(2,1)} %bitcast.30, ...), custom_call_target="tpu_custom_call" | custom-call | tf_op jit(solution)/shard_map/moe_exchange/pallas_call | solution.py:259
  90.5 1.7 %copy.29 = bf16[64,2048]{1,0:T(8,128)(2,1)} copy(bf16[64,2048]{1,0:T(8,128)(2,1)} %moe_exchange.1) | data formatting | bytes 524288
  (3 shorter events, 0.0 us)
Async XLA Ops:
  5.1 10.2 %copy-start = (s32[64,6]{0,1:T(8,128)S(1)}, s32[64,6]{0,1:T(8,128)}, u32[]{:S(2)}) copy-start(s32[64,6]{0,1:T(8,128)} %param.42) | copy-start | bytes 4612
  5.1 10.2 %copy-start.1 = (f32[64,6]{0,1:T(8,128)S(1)}, f32[64,6]{0,1:T(8,128)}, u32[]{:S(2)}) copy-start(f32[64,6]{0,1:T(8,128)} %param.43) | copy-start | bytes 4612
